TPU v7x, 256 devices: a whole 4x4x8 slice. The times are simulated.
256 devices in a mesh: dp: 4 (over y), kv: 32 (over z, x), tp: 2 (over core).
Axes of the slice: x: 4, y: 4, z: 8, core: 2. Of those that a mesh axis runs over, the one named last changes fastest.
Arguments:
- tokens: bfloat16 [32768, 2048], P(('dp', 'kv'), 'tp'), parts along dimension 0, may hold values from -6 to 6
- query_weight: bfloat16 [2048, 1024], P(None, 'tp'), may hold values from -2 to 2
- key_weight: bfloat16 [2048, 1024], P(None, 'tp'), may hold values from -2 to 2
- value_weight: bfloat16 [2048, 1024], P(None, 'tp'), may hold values from -0.125 to 0.125
- out_weight: bfloat16 [1024, 2048], P(None, 'tp'), may hold values from -0.75 to 0.75
- chosen: int32 [1024, 16], P(('dp', 'kv')), parts along dimension 0, may hold values from -1 to 255, as said below
Outputs:
- mixed: bfloat16 [32768, 2048], P(('dp', 'kv'), 'tp'), parts along dimension 0
There are 4 independent parts, one for each index of `dp`. A program takes and returns all parts, laid end to end along the dimension named above; an argument that names none is the same for every part. Nothing has to cross between parts.
Inputs may be any that keep to these rules, and one draw needn't show every extreme that they name: Each row of chosen lists distinct key blocks no later than its own query block, followed or mixed with -1 for empty slots; the own block is always listed, and block 0 too. For the 8 query blocks of one index of kv (aligned runs of rows), the distinct listed key blocks that lie among the 8 blocks of any one other index number at most 3, and exactly 3 for the index just before.
All inputs are finite; a program needn't handle non-finite values.
Results may differ from a plain program's by a relative error of at most 0.0084.
Values may be sent and summed in bfloat16 or wider, within the bound.
A program may use at most 128 MiB of HBM per device.

v0:
```python
import jax
import jax.numpy as jnp
from jax import lax
from jax.sharding import Mesh
from jax.sharding import PartitionSpec as P

HEAD_DIM = 64
BLOCK = 32
CAP = 3
KV = ("kv_0", "kv_1")
DP_KV = ("dp", "kv_0", "kv_1")


rotary_base = 500000.0
masked_score = -1e30


def copy_for_each(x, axis):
    copies = jnp.broadcast_to(x, (lax.axis_size(axis), *x.shape))
    return lax.all_to_all(copies, axis, split_axis=0, concat_axis=0, tiled=True)


def in_order(tiles, dim):
    tiles = jnp.moveaxis(tiles, 0, dim)
    dims = tiles.shape
    return tiles.reshape(*dims[:dim], dims[dim] * dims[dim + 1], *dims[dim + 2 :])


def gathered_copies(x, axis, dim):
    tiles = copy_for_each(x, axis)
    return in_order(tiles, dim)


def cut_along(x, dim, devices):
    before, after = (x.shape[:dim], x.shape[dim + 1 :])
    return jnp.moveaxis(x.reshape(*before, devices, -1, *after), dim, 0)


def moved_by_axis(tiles, axes, sequence):
    inside = tiles.shape[1:]
    whole = tiles.reshape(*(lax.axis_size(a) for a in axes), *inside)
    for k in sequence:
        whole = lax.all_to_all(whole, axes[k], k, k, tiled=True)
    return whole.reshape(-1, *inside)


def exchange_by_axis(x, axes, sequence, split_dim, concat_dim):
    tiles = cut_along(x, split_dim, lax.axis_size(axes))
    return in_order(moved_by_axis(tiles, axes, sequence), concat_dim)


def rotate(heads_in, positions):
    half_dim = heads_in.shape[-1] // 2
    inverse = 1.0 / rotary_base ** (jnp.arange(half_dim, dtype=jnp.float32) / half_dim)
    angles = positions.astype(jnp.float32)[:, None] * inverse[None, :]
    cosine = jnp.cos(angles)[:, None, :]
    sine_part = jnp.sin(angles)[:, None, :]
    first_half = heads_in[..., :half_dim]
    second_half = heads_in[..., half_dim:]
    return jnp.concatenate(
        [
            first_half * cosine - second_half * sine_part,
            first_half * sine_part + second_half * cosine,
        ],
        axis=-1,
    )


def attend_keys(
    carried, queries, key_rows, value_rows, key_block, key_pos, key_valid, listed, query_pos
):
    key_count = key_rows.shape[0]
    head_count = queries.shape[0]
    hit_mask = jnp.any(listed[:, :, None] == key_block[None, None, :], axis=1)
    hit_mask = jnp.repeat(hit_mask, BLOCK, axis=0)
    allowed = hit_mask & key_valid[None, :] & (key_pos[None, :] <= query_pos[:, None])
    keys_heads = key_rows.reshape(key_count, head_count, HEAD_DIM).transpose(1, 0, 2)
    values_heads = value_rows.reshape(key_count, head_count, HEAD_DIM).transpose(1, 0, 2)
    score_scale = HEAD_DIM ** (-0.5)

    def one_head(inputs):
        query_head, key_head, value_head, peak_now, denominator, summed = inputs
        scores = (
            jnp.einsum("qd,kd->qk", query_head, key_head, preferred_element_type=jnp.float32)
            * score_scale
        )
        scores = jnp.where(allowed, scores, masked_score)
        peak_new = jnp.maximum(peak_now, jnp.max(scores, axis=1))
        factor = jnp.exp(peak_now - peak_new)
        weights = jnp.where(allowed, jnp.exp(scores - peak_new[:, None]), 0.0)
        denominator = denominator * factor + jnp.sum(weights, axis=1)
        summed = summed * factor[:, None] + jnp.dot(
            weights.astype(jnp.bfloat16), value_head, preferred_element_type=jnp.float32
        )
        return (peak_new, denominator, summed)

    peak_now, denominator, summed = carried
    return lax.map(one_head, (queries, keys_heads, values_heads, peak_now, denominator, summed))


def on_device(tokens, query_weight, key_weight, value_weight, out_weight, chosen):
    row_count = tokens.shape[0]
    head_width = query_weight.shape[1]
    head_count = head_width // HEAD_DIM
    device = lax.axis_index(KV)
    devices = lax.axis_size(KV)
    blocks_dev = row_count // BLOCK
    query_pos = device * row_count + jnp.arange(row_count, dtype=jnp.int32)
    fragment = gathered_copies(tokens, "tp", 1)
    query_acc, key_acc, value_acc = tuple(
        (
            jnp.dot(fragment, weight, preferred_element_type=jnp.float32)
            for weight in (query_weight, key_weight, value_weight)
        )
    )
    heads_shape = (row_count, head_count, HEAD_DIM)
    query_proj = rotate(query_acc.reshape(heads_shape), query_pos).astype(jnp.bfloat16)
    key_proj = (
        rotate(key_acc.reshape(heads_shape), query_pos)
        .astype(jnp.bfloat16)
        .reshape(row_count, head_width)
    )
    value_proj = value_acc.astype(jnp.bfloat16)
    queries = query_proj.transpose(1, 0, 2)
    start_state = (
        jnp.full((head_count, row_count), masked_score, jnp.float32),
        jnp.zeros((head_count, row_count), jnp.float32),
        jnp.zeros((head_count, row_count, HEAD_DIM), jnp.float32),
    )
    block_ids = jnp.arange(devices * blocks_dev, dtype=jnp.int32)
    needed = jnp.any(chosen.reshape(-1)[:, None] == block_ids[None, :], axis=0)
    needed = needed & (block_ids // blocks_dev != device)
    need_grid = needed.reshape(devices, blocks_dev).astype(jnp.int32)
    rank_in = jnp.cumsum(need_grid, axis=1) - need_grid
    slot_hit = (need_grid[:, None, :] == 1) & (
        rank_in[:, None, :] == jnp.arange(CAP, dtype=jnp.int32)[None, :, None]
    )
    request = jnp.sum(
        slot_hit.astype(jnp.int32) * jnp.arange(blocks_dev, dtype=jnp.int32)[None, None, :], axis=2
    )
    present = jnp.any(slot_hit, axis=2)
    incoming = exchange_by_axis(request, KV, (0, 1), 0, 0)
    key_store = key_proj.reshape(blocks_dev, BLOCK, head_width)
    value_store = value_proj.reshape(blocks_dev, BLOCK, head_width)
    got_keys, got_values = (
        lax.all_to_all(key_store[incoming], KV, split_axis=0, concat_axis=0, tiled=True),
        lax.all_to_all(value_store[incoming], KV, split_axis=0, concat_axis=0, tiled=True),
    )
    remote_block = jnp.arange(devices, dtype=jnp.int32)[:, None] * blocks_dev + request
    remote_pos = (
        remote_block[:, :, None] * BLOCK + jnp.arange(BLOCK, dtype=jnp.int32)[None, None, :]
    ).reshape(-1)
    remote_valid = jnp.broadcast_to(present[:, :, None], (devices, CAP, BLOCK)).reshape(-1)
    key_rows = jnp.concatenate([key_proj, got_keys.reshape(-1, head_width)], axis=0)
    value_rows = jnp.concatenate([value_proj, got_values.reshape(-1, head_width)], axis=0)
    key_pos = jnp.concatenate([query_pos, remote_pos])
    key_valid = jnp.concatenate([jnp.ones((row_count,), jnp.bool_), remote_valid])
    peak_now, denominator, summed = attend_keys(
        start_state,
        queries,
        key_rows,
        value_rows,
        key_pos // BLOCK,
        key_pos,
        key_valid,
        chosen,
        query_pos,
    )
    attended = (
        (summed / denominator[:, :, None])
        .astype(jnp.bfloat16)
        .transpose(1, 0, 2)
        .reshape(row_count, head_width)
    )
    mixed = jnp.dot(
        gathered_copies(attended, "tp", 1), out_weight, preferred_element_type=jnp.float32
    )
    return mixed.astype(jnp.bfloat16)


def solution(mesh):
    torus = Mesh(
        mesh.devices.reshape(mesh.shape["dp"], 8, 4, mesh.shape["tp"]), ("dp", "kv_0", "kv_1", "tp")
    )
    placed = (
        P(DP_KV, "tp"),
        P(None, "tp"),
        P(None, "tp"),
        P(None, "tp"),
        P(None, "tp"),
        P(DP_KV, None),
    )
    return jax.shard_map(
        on_device, mesh=torus, in_specs=placed, out_specs=P(DP_KV, "tp"), check_vma=False
    )
```

profile of v0, /device:TPU:1, one launch (start us, length us, event | category | flops | bytes accessed | tf_op | source)
XLA Modules:
  0.0 276.1 jit_solution(12876118896892895078)
XLA Ops:
  0.0 2.3 broadcast_in_dim.18
  2.3 6.8 %all-to-all-start = ((bf16[2,256,1024]{2,1,0:T(8,128)(2,1)}), bf16[2,256,1024]{2,1,0:T(8,128)(2,1)S(1)}, u32[]{:S(2)}, u32[]{:S(2)}) async-start(bf16[2,256,1024]{2,1,0:T(8,128)(2,1)} %broadcast_in_dim.18), calls=%async_computation | async-start | bytes 2097152 | tf_op jit(solution)/shard_map/all_to_all | solution.py:20
  11.0 6.5 %all-to-all-start.1 = ((s32[8,4,1,3]{1,2,3,0:T(1,128)}), s32[8,4,1,3]{1,2,3,0:T(1,128)S(1)}, u32[]{:S(2)}, u32[]{:S(2)}) async-start(s32[8,4,1,3]{1,2,3,0:T(1,128)} %copy.62), calls=%async_computation.1 | async-start | bytes 24576 | tf_op jit(solution)/shard_map/all_to_all | solution.py:43
  19.6 2.6 reshape.379
  22.2 4.0 %copy.58 = bf16[2048,512]{0,1:T(8,128)(2,1)} copy(bf16[2048,512]{1,0:T(8,128)(2,1)} %param.10) | data formatting | bytes 4194304 | tf_op args[2]
  26.4 2.7 fusion.44
  30.5 4.0 %all-to-all-start.2 = ((s32[8,4,1,3]{0,2,3,1:T(1,128)}), s32[8,4,1,3]{0,2,3,1:T(1,128)S(1)}, u32[]{:S(2)}, u32[]{:S(2)}) async-start(s32[8,4,1,3]{0,2,3,1:T(1,128)} %copy.63), calls=%async_computation.2 | async-start | bytes 12288 | tf_op jit(solution)/shard_map/all_to_all | solution.py:43
  39.1 2.5 gather_fusion
  41.6 9.1 %all-to-all-start.3 = ((bf16[32,3,32,512]{3,2,1,0:T(8,128)(2,1)}), bf16[32,3,32,512]{3,2,1,0:T(8,128)(2,1)}, u32[]{:S(2)}, u32[]{:S(2)}) async-start(bf16[32,3,32,512]{3,2,1,0:T(8,128)(2,1)} %bitcast.86), calls=%async_computation.3 | async-start | bytes 6291456 | tf_op jit(solution)/shard_map/all_to_all | solution.py:146
  50.8 2.3 convolution_convert_fusion.1
  53.1 2.6 gather_fusion.1
  55.6 66.0 %all-to-all-done.3 = bf16[32,3,32,512]{3,2,1,0:T(8,128)(2,1)} async-done(((bf16[32,3,32,512]{3,2,1,0:T(8,128)(2,1)}), bf16[32,3,32,512]{3,2,1,0:T(8,128)(2,1)}, u32[]{:S(2)}, u32[]{:S(2)}) %all-to-all-start.3) | async-done | bytes 3145760 | tf_op jit(solution)/shard_map/all_to_all | solution.py:146
  121.7 6.7 %all-to-all-start.4 = ((bf16[32,3,32,512]{3,2,1,0:T(8,128)(2,1)}), bf16[32,3,32,512]{3,2,1,0:T(8,128)(2,1)}, u32[]{:S(2)}, u32[]{:S(2)}) async-start(bf16[32,3,32,512]{3,2,1,0:T(8,128)(2,1)} %bitcast.85), calls=%async_computation.4 | async-start | bytes 6291456 | tf_op jit(solution)/shard_map/all_to_all | solution.py:147
  128.5 4.0 %copy.57 = bf16[2048,512]{0,1:T(8,128)(2,1)} copy(bf16[2048,512]{1,0:T(8,128)(2,1)} %param.9) | data formatting | bytes 4194304 | tf_op args[1]
  133.5 2.7 fusion.43
  136.8 9.0 %concatenate.42 = bf16[3072,8,64]{2,1,0:T(8,128)(2,1)} reshape(bf16[32,3,32,512]{3,2,1,0:T(8,128)(2,1)} %all-to-all-done.3) | data formatting | bytes 6291456 | tf_op jit(solution)/shard_map/concatenate | solution.py:154
  145.7 6.4 %maximum_bitcast_fusion = bf16[8,3328,64]{2,0,1:T(8,128)(2,1)S(1)} fusion(bf16[3072,8,64]{2,1,0:T(8,128)(2,1)} %concatenate.42, bf16[256,8,64]{2,1,0:T(8,128)(2,1)S(1)} %copy-done.1), kind=kLoop, calls=%fused_computation.28 | loop fusion | flops 1703936 | bytes 6815744 | tf_op jit(solution)/shard_map/transpose | solution.py:77
  152.1 3.9 %copy.72 = bf16[8,3328,64]{2,1,0:T(8,128)(2,1)} copy(bf16[8,3328,64]{2,0,1:T(8,128)(2,1)S(1)} %maximum_bitcast_fusion) | data formatting | bytes 6815744
  156.1 41.7 %all-to-all-done.4 = bf16[32,3,32,512]{3,2,1,0:T(8,128)(2,1)} async-done(((bf16[32,3,32,512]{3,2,1,0:T(8,128)(2,1)}), bf16[32,3,32,512]{3,2,1,0:T(8,128)(2,1)}, u32[]{:S(2)}, u32[]{:S(2)}) %all-to-all-start.4) | async-done | bytes 3145760 | tf_op jit(solution)/shard_map/all_to_all | solution.py:147
  197.7 8.9 %concatenate.47 = bf16[3072,8,64]{2,1,0:T(8,128)(2,1)} reshape(bf16[32,3,32,512]{3,2,1,0:T(8,128)(2,1)} %all-to-all-done.4) | data formatting | bytes 6291456 | tf_op jit(solution)/shard_map/concatenate | solution.py:155
  206.7 6.4 %maximum_bitcast_fusion.1 = bf16[8,3328,64]{2,0,1:T(8,128)(2,1)S(1)} fusion(bf16[3072,8,64]{2,1,0:T(8,128)(2,1)} %concatenate.47, bf16[256,8,64]{2,1,0:T(8,128)(2,1)S(1)} %copy.68), kind=kLoop, calls=%fused_computation.29 | loop fusion | flops 1703936 | bytes 6815744 | tf_op jit(solution)/shard_map/transpose | solution.py:78
  213.1 4.0 %copy.73 = bf16[8,3328,64]{2,1,0:T(8,128)(2,1)} copy(bf16[8,3328,64]{2,0,1:T(8,128)(2,1)S(1)} %maximum_bitcast_fusion.1) | data formatting | bytes 6815744
  217.1 49.9 %while.13 = (s32[]{:T(128)}, f32[8,256]{1,0:T(8,128)S(1)}, f32[8,256,64]{1,2,0:T(8,128)S(1)}, bf16[8,256,64]{1,2,0:T(8,128)(2,1)S(1)}, bf16[8,3328,64]{2,1,0:T(8...) while((s32[]{:T(128)}, f32[8,256]{1,0:T(8,128)S(1)}, ...), condition=%wide.region_8.9_spmd.clone, body=%wide.region_5.8_spmd.clone.sunk | while | flops 230900480 | bytes 14685817 | solution.py:98
  221.1 2.1 fusion.64
  227.3 2.1 fusion.64
  233.6 2.1 fusion.64
  239.8 2.1 fusion.64
  246.0 2.1 fusion.64
  252.3 2.1 fusion.64
  258.5 2.1 fusion.64
  264.8 2.1 fusion.64
  267.1 7.5 %all_to_all.30 = bf16[2,256,512]{1,2,0:T(8,128)(2,1)S(1)} all-to-all(bf16[2,256,512]{1,2,0:T(8,128)(2,1)S(1)} %broadcast_in_dim.21), channel_id=1, replica_groups=mesh['dp'=4,'kv_0'=8,'kv_1'=4,'tp'=2] {'tp'}, dimensions={0} | all-to-all | bytes 1048576 | tf_op jit(solution)/shard_map/all_to_all | solution.py:20
  (125 shorter events, 45.9 us)
Async XLA Ops:
  0.0 274.6 %copy-start = (bf16[1024,1024]{1,0:T(8,128)(2,1)S(1)}, bf16[1024,1024]{1,0:T(8,128)(2,1)}, u32[]{:S(2)}) copy-start(bf16[1024,1024]{1,0:T(8,128)(2,1)} %param.12) | copy-start | bytes 6291460
  0.0 9.1 %copy-start.9 = (s32[8,16]{1,0:T(8,128)S(1)}, s32[8,16]{1,0:T(8,128)}, u32[]{:S(2)}) copy-start(s32[8,16]{1,0:T(8,128)} %param.13) | copy-start | bytes 1540
  2.3 8.7 %all-to-all-start = ((bf16[2,256,1024]{2,1,0:T(8,128)(2,1)}), bf16[2,256,1024]{2,1,0:T(8,128)(2,1)S(1)}, u32[]{:S(2)}, u32[]{:S(2)}) async-start(bf16[2,256,1024]{2,1,0:T(8,128)(2,1)} %broadcast_in_dim.18), calls=%async_computation | async-start | bytes 2097152 | tf_op jit(solution)/shard_map/all_to_all | solution.py:20
  9.8 0.6 copy-start.11
  10.3 15.8 %copy-start.7 = (s32[32,3]{0,1:T(4,128)}, s32[32,3]{0,1:T(4,128)S(1)}, u32[]{:S(2)}) copy-start(s32[32,3]{0,1:T(4,128)S(1)} %select_reduce_fusion) | copy-start | bytes 1156
  11.0 18.8 %all-to-all-start.1 = ((s32[8,4,1,3]{1,2,3,0:T(1,128)}), s32[8,4,1,3]{1,2,3,0:T(1,128)S(1)}, u32[]{:S(2)}, u32[]{:S(2)}) async-start(s32[8,4,1,3]{1,2,3,0:T(1,128)} %copy.62), calls=%async_computation.1 | async-start | bytes 24576 | tf_op jit(solution)/shard_map/all_to_all | solution.py:43
  26.3 2.7 copy-start.3
  26.4 2.7 copy-start.5
  30.5 8.2 %all-to-all-start.2 = ((s32[8,4,1,3]{0,2,3,1:T(1,128)}), s32[8,4,1,3]{0,2,3,1:T(1,128)S(1)}, u32[]{:S(2)}, u32[]{:S(2)}) async-start(s32[8,4,1,3]{0,2,3,1:T(1,128)} %copy.63), calls=%async_computation.2 | async-start | bytes 12288 | tf_op jit(solution)/shard_map/all_to_all | solution.py:43
  41.6 80.1 %all-to-all-start.3 = ((bf16[32,3,32,512]{3,2,1,0:T(8,128)(2,1)}), bf16[32,3,32,512]{3,2,1,0:T(8,128)(2,1)}, u32[]{:S(2)}, u32[]{:S(2)}) async-start(bf16[32,3,32,512]{3,2,1,0:T(8,128)(2,1)} %bitcast.86), calls=%async_computation.3 | async-start | bytes 6291456 | tf_op jit(solution)/shard_map/all_to_all | solution.py:146
  121.7 76.1 %all-to-all-start.4 = ((bf16[32,3,32,512]{3,2,1,0:T(8,128)(2,1)}), bf16[32,3,32,512]{3,2,1,0:T(8,128)(2,1)}, u32[]{:S(2)}, u32[]{:S(2)}) async-start(bf16[32,3,32,512]{3,2,1,0:T(8,128)(2,1)} %bitcast.85), calls=%async_computation.4 | async-start | bytes 6291456 | tf_op jit(solution)/shard_map/all_to_all | solution.py:147
  128.3 4.2 %copy-start.8 = (s32[32,3]{0,1:T(4,128)S(1)}, s32[32,3]{0,1:T(4,128)}, u32[]{:S(2)}) copy-start(s32[32,3]{0,1:T(4,128)} %copy-done.7) | copy-start | bytes 1156
  128.3 4.8 %copy-start.12 = (pred[32,8]{0,1:T(8,128)(4,1)S(1)}, pred[32,8]{0,1:T(8,128)(4,1)}, u32[]{:S(2)}) copy-start(pred[32,8]{0,1:T(8,128)(4,1)} %copy-done.11) | copy-start | bytes 772
  132.5 3.7 %copy-start.4 = (f32[256,32]{0,1:T(8,128)S(1)}, f32[256,32]{0,1:T(8,128)}, u32[]{:S(2)}) copy-start(f32[256,32]{0,1:T(8,128)} %copy-done.3) | copy-start | bytes 98308
  132.5 3.7 %copy-start.6 = (f32[256,32]{0,1:T(8,128)S(1)}, f32[256,32]{0,1:T(8,128)}, u32[]{:S(2)}) copy-start(f32[256,32]{0,1:T(8,128)} %copy-done.5) | copy-start | bytes 98308
  132.5 3.8 %copy-start.10 = (s32[8,16]{1,0:T(8,128)S(1)}, s32[8,16]{1,0:T(8,128)}, u32[]{:S(2)}) copy-start(s32[8,16]{1,0:T(8,128)} %param.13) | copy-start | bytes 1540
  136.7 9.0 %copy-start.1 = (bf16[256,8,64]{2,1,0:T(8,128)(2,1)S(1)}, bf16[256,8,64]{2,1,0:T(8,128)(2,1)}, u32[]{:S(2)}) copy-start(bf16[256,8,64]{2,1,0:T(8,128)(2,1)} %copy.66) | copy-start | bytes 786436
  213.1 4.0 %copy-start.2 = (f32[8,256,64]{1,2,0:T(8,128)S(1)}, f32[8,256,64]{1,2,0:T(8,128)}, u32[]{:S(2)}) copy-start(f32[8,256,64]{1,2,0:T(8,128)} %custom-call.5) | copy-start | bytes 1572868
where the time goes:
time: 278 us; the launch traced here: 276 us
  waiting for transfers between devices  108 us (39%)
  local copies, waits for them, and re-layouts  52.3 us (19%)
  matrix products  42.7 us (15%)
  starting transfers between devices  33 us (12%)
  other arithmetic  31.5 us (11%)
  blocking collectives  7.48 us (3%)
    all_to_all x1, waiting for transfers between devices, on_device(): lax.all_to_all(key_store[incoming], KV, split_axis=0, concat_axis=0, tile...  66 us
    all_to_all x1, waiting for transfers between devices, on_device(): lax.all_to_all(value_store[incoming], KV, split_axis=0, concat_axis=0, ti...  41.7 us
    dot_general x8, matrix products, one_head(): jnp.dot(weights.astype(jnp.bfloat16), value_head, preferred_element_type=...  17.1 us
    unnamed x30, local copies, waits for them, and re-layouts  16.4 us
    dot_general x8, matrix products, one_head(): jnp.einsum('qd,kd->qk', query_head, key_head, preferred_element_type=jnp....  16.4 us
    all_to_all x2, starting transfers between devices, moved_by_axis(): whole = lax.all_to_all(whole, axes[k], k, k, tiled=True)  10.5 us
    reduce_sum x8, other arithmetic, one_head(): denominator = denominator * factor + jnp.sum(weights, axis=1)  10.1 us
    concatenate x2, local copies, waits for them, and re-layouts, on_device(): jnp.concatenate([value_proj, got_values.reshape(-1, head_width)], axis=0)  9.22 us
  transfers between devices with their start and end apart: 5, of which 3 were waited for; matrix products, arithmetic and copies ran while one was open for 18% of the time, Pallas kernels for 0%

commit v1 on v0

v1 whole, which is shorter than its diff:
```python
import functools

import jax
import jax.numpy as jnp
import numpy as np
from jax import lax
from jax.experimental import pallas as pl
from jax.experimental.pallas import tpu as pltpu
from jax.sharding import PartitionSpec as P

DP_KV = ("dp", "kv")
MESH = pl.DeviceIdType.MESH

HEAD_DIM = 64
BLOCK = 32
CAP = 3
ROWS = 256
QB = 8
XS = 4
ZS = 8
SRC = 8
PAIR = 128
LISTED = CAP * SRC * BLOCK
OUT_KEYS = SRC * BLOCK
HP = 4
SLOTS = 3
MASKED = -1e30
ROTARY_BASE = 500000.0


def tables():
    lane = np.arange(PAIR)
    inverse = ROTARY_BASE ** (-(lane % 32) / 32.0)
    inside = np.arange(ROWS)[:, None] * inverse[None, :]
    device = (np.arange(XS * ZS) * ROWS)[:, None] * inverse[None, :]
    row_table = np.stack([np.cos(inside), np.sin(inside)]).astype(np.float32)
    device_table = np.zeros((XS * ZS, 8, PAIR), np.float32)
    device_table[:, 0] = np.cos(device)
    device_table[:, 1] = np.sin(device)
    return row_table, device_table


def iota(shape, dim):
    return lax.broadcasted_iota(jnp.int32, shape, dim)


def half_scores(q, keys, half):
    q_half = q * half
    return lax.dot_general(
        q_half, keys, (((1,), (1,)), ((), ())), preferred_element_type=jnp.float32
    )


def attend(q, keys, values, bias):
    lane = iota((1, PAIR), 1)
    first = (lane < HEAD_DIM).astype(jnp.float32)
    halves = (first.astype(jnp.bfloat16), (1.0 - first).astype(jnp.bfloat16))
    outs, peaks = [], []
    for half, other in (halves, halves[::-1]):
        scores = half_scores(q, keys, half)
        scores = bias(scores)
        peak = jnp.max(scores, axis=1, keepdims=True)
        weight = jnp.exp(scores - peak).astype(jnp.bfloat16)
        outs.append(
            jnp.dot(weight, values * half + other, preferred_element_type=jnp.float32)
        )
        peaks.append(peak)
    in_first = iota((ROWS, PAIR), 1) < HEAD_DIM
    numerator = jnp.where(in_first, outs[0], outs[1])
    sums = pltpu.roll(jnp.where(in_first, outs[1], outs[0]), HEAD_DIM, 1)
    peak = jnp.where(in_first, peaks[0], peaks[1])
    return numerator, sums, peak


def compact(peak, sums):
    lane = iota((ROWS, PAIR), 1)
    turned = jnp.where(lane % HEAD_DIM < 32, peak, sums).T
    row = iota((8, ROWS), 0) % 4
    return jnp.where(
        row == 0,
        turned[0:8],
        jnp.where(row == 1, turned[32:40], jnp.where(row == 2, turned[64:72], turned[96:104])),
    )


def kernel(
    tok_hbm, wq_hbm, wk_hbm, wv_hbm, ow_hbm, ch_hbm, tab_hbm, dev_hbm, out_hbm, *scratch
):
    kv = scratch[:HP]
    (
        tok, wq, wk, wv, ow, ch, tab, dev, angle, acc, listing, own_bias, pair_bias, table,
        got_bias, got_table, q_buf, o_out, s_out, o_in, s_in, own_o, own_s, att, out_buf, small,
        load_sem, send, recv, tok_sem, q_send, q_recv, m_send, m_recv, o_send, o_recv,
        s_send, s_recv, small_sem, out_sem,
    ) = scratch[HP:]
    dp, me, core = (lax.axis_index(a) for a in ("dp", "kv", "tp"))
    z, x = me // XS, me % XS
    pair, odd = z // 2, z % 2
    left, right = (x + XS - 1) % XS, (x + 1) % XS
    other_row = z + 1 - 2 * odd
    half_d = tok.shape[2]
    width = wq.shape[1]

    def at(row, column):
        return (dp, row * XS + column, core)

    mate = (dp, me, 1 - core)

    loads = [
        (tok_hbm, tok.at[core]), (wk_hbm, wk), (wv_hbm, wv), (wq_hbm, wq), (ch_hbm, ch),
        (tab_hbm, tab), (dev_hbm, dev), (ow_hbm, ow),
    ]
    loads = [
        pltpu.make_async_copy(a, b, load_sem.at[i]) for i, (a, b) in enumerate(loads)
    ]
    for i in (4, 0, 1, 2, 3, 5, 6, 7):
        loads[i].start()

    barrier = pltpu.get_barrier_semaphore()

    def greet(device):
        pl.semaphore_signal(barrier, inc=1, device_id=device, device_id_type=MESH)

    greet(mate)
    greet(at(z, left))
    greet(at(z, right))
    for k in range(1, ZS):
        greet(at((z + k) % ZS, x))

    loads[4].wait()
    lane = iota((QB, ROWS), 1)
    lane8 = lane % QB
    chosen = ch[...]
    hit = jnp.zeros((QB, ROWS), jnp.int32)
    for t in range(chosen.shape[1]):
        hit = jnp.where(chosen[:, t : t + 1] == lane, 1, hit)
    need = jnp.max(hit, axis=0, keepdims=True)
    need = jnp.broadcast_to(need, (QB, ROWS))
    need = jnp.where(lane // QB == me, 0, need)
    rank = need
    for k in (1, 2, 4):
        rank = rank + jnp.where(lane8 >= k, pltpu.roll(rank, k, 1), 0)
    rank = rank - need
    sub = iota((QB, ROWS), 0)
    listed = jnp.zeros((QB, ROWS), jnp.int32)
    placed = []
    for slot in range(CAP):
        here = jnp.where(rank == slot, need, 0)
        placed.append((hit * here).astype(jnp.float32))
        where = here * lane8
        for k in (1, 2, 4):
            where = where + jnp.where(lane8 >= k, pltpu.roll(where, k, 1), 0)
        listed = jnp.where(sub == slot, where, listed)
    table[...] = listed
    placed = jnp.concatenate(placed, axis=0).astype(jnp.bfloat16)
    for k in range(4):
        spread = (iota((ROWS, OUT_KEYS), 0) // QB) == (iota((ROWS, OUT_KEYS), 1) // BLOCK + k * SRC)
        spread = spread.astype(jnp.float32).astype(jnp.bfloat16)
        found = jnp.dot(placed, spread, preferred_element_type=jnp.float32)
        pair_bias[k] = (found - 1.0) * -MASKED
    spread = iota((ROWS, ROWS), 0) == (iota((ROWS, ROWS), 1) // BLOCK + me * QB)
    spread = spread.astype(jnp.float32).astype(jnp.bfloat16)
    found = jnp.dot(
        hit.astype(jnp.float32).astype(jnp.bfloat16), spread, preferred_element_type=jnp.float32
    )
    listing[...] = (found - 1.0) * -MASKED
    for b in range(QB):
        rows = pl.ds(b * BLOCK, BLOCK)
        causal = iota((BLOCK, ROWS), 1) <= iota((BLOCK, ROWS), 0) + b * BLOCK
        own_bias[rows, :] = jnp.where(causal, listing[b : b + 1, :], MASKED)

    loads[5].wait()
    loads[6].wait()
    dev_cos, dev_sin = dev[me, 0:1, :], dev[me, 1:2, :]
    sign = jnp.where(iota((1, PAIR), 1) % HEAD_DIM < 32, -1.0, 1.0)
    angle[0] = tab[0] * dev_cos - tab[1] * dev_sin
    angle[1] = (tab[1] * dev_cos + tab[0] * dev_sin) * sign

    for k in range(SLOTS):
        @pl.when(pair <= k)
        def _():
            for hp in range(HP):
                o_in[hp, k] = jnp.zeros((ROWS, PAIR), jnp.bfloat16)
                s_in[hp, k] = jnp.full((8, ROWS), MASKED, jnp.float32)

    def remote(src, dst, send_sem, recv_sem, device):
        return pltpu.make_async_remote_copy(
            src_ref=src, dst_ref=dst, send_sem=send_sem, recv_sem=recv_sem,
            device_id=device, device_id_type=MESH,
        )

    pl.semaphore_wait(barrier, 3 + ZS - 1)
    loads[0].wait()
    tokens = remote(tok.at[core], tok.at[core], tok_sem.at[0], tok_sem.at[1], mate)
    tokens.start()

    for w, load in ((0, 1), (1, 2), (2, 3)):
        loads[load].wait()
        weight = (wk, wv, wq)[w]
        for c in range(width // 256):
            cols = pl.ds(c * 256, 256)
            acc[w, c] = jnp.dot(
                tok[core], weight[pl.ds(core * half_d, half_d), cols],
                preferred_element_type=jnp.float32,
            )
    theirs = remote(tok.at[1 - core], tok.at[1 - core], tok_sem.at[0], tok_sem.at[1], mate)
    theirs.wait_recv()

    def project(w, c):
        weight = (wk, wv, wq)[w]
        cols = pl.ds(c * 256, 256)
        return acc[w, c] + jnp.dot(
            tok[1 - core], weight[pl.ds((1 - core) * half_d, half_d), cols],
            preferred_element_type=jnp.float32,
        )

    low = iota((ROWS, PAIR), 1) % HEAD_DIM < 32

    def turn(part):
        partner = jnp.where(low, pltpu.roll(part, PAIR - 32, 1), pltpu.roll(part, 32, 1))
        return part * angle[0] + partner * angle[1]

    def blocked(part):
        return part.astype(jnp.bfloat16).reshape(QB, BLOCK, PAIR)

    own = odd * XS + x
    mated = (1 - odd) * XS + x
    far = (x + 2) % XS

    def hop(kind, hp, source, device, which=None):
        part = kv[hp].at[source] if which is None else kv[hp].at[source, which]
        return remote(part, part, send.at[kind, hp], recv.at[kind, hp], device)

    def send_own(hp):
        hop(1, hp, own, at(z, right)).start()
        hop(2, hp, own, at(z, left)).start()

    def send_across(hp):
        hop(0, hp, own, at(other_row, x)).start()

    q_row = [1 - z // 5, 3 - z // 7, z * 0 + 5]
    q_slot = [(z + 1) % 3, (z + 2) % 3, z % 2]

    def q_copy(k, hp, slot):
        return remote(
            q_buf.at[hp, SLOTS], q_buf.at[hp, slot], q_send.at[k, hp], q_recv.at[slot, hp],
            at(q_row[k], x),
        )

    def meta_copies(k, slot):
        return (
            remote(pair_bias.at[k], got_bias.at[slot], m_send.at[k, 0], m_recv.at[slot, 0],
                   at(q_row[k], x)),
            remote(table, got_table.at[slot], m_send.at[k, 1], m_recv.at[slot, 1],
                   at(q_row[k], x)),
        )

    for c in range(width // 256):
        keys, values = project(0, c), project(1, c)
        for i in range(2):
            hp = 2 * c + i
            part = slice(i * PAIR, (i + 1) * PAIR)
            kv[hp][own, 0] = blocked(turn(keys[:, part]))
            kv[hp][own, 1] = blocked(values[:, part])
            send_across(hp)
            if hp < 2:
                send_own(hp)
    for c in range(width // 256):
        queries = project(2, c)
        for i in range(2):
            hp = 2 * c + i
            part = slice(i * PAIR, (i + 1) * PAIR)
            turned = turn(queries[:, part]).astype(jnp.bfloat16).astype(jnp.float32)
            q_buf[hp, SLOTS] = (turned * HEAD_DIM**-0.5).astype(jnp.bfloat16)
            for k in range(SLOTS):
                @pl.when(pair > k)
                def _():
                    if hp == 0:
                        for copy in meta_copies(k, q_slot[k]):
                            copy.start()
                    q_copy(k, hp, q_slot[k]).start()

    own_small = pltpu.make_async_copy(table, small.at[SLOTS], small_sem.at[SLOTS])
    own_small.start()

    own_left, own_right, own_far = odd * XS + left, odd * XS + right, odd * XS + far
    row2 = (1 - odd) * XS
    mate_left, mate_right, mate_far = row2 + left, row2 + right, row2 + far

    def pass_mate(hp):
        hop(0, hp, mated, at(other_row, x)).wait_recv()
        hop(3, hp, mated, at(z, right)).start()
        hop(4, hp, mated, at(z, left)).start()

    def relay_own(hp):
        hop(1, hp, own_left, at(z, right)).wait_recv()
        hop(5, hp, own_left, at(z, right), 0).start()
        hop(2, hp, own_right, at(z, left)).wait_recv()
        hop(6, hp, own_right, at(z, left), 1).start()

    def relay_mate(hp):
        hop(3, hp, mate_left, at(z, right)).wait_recv()
        hop(7, hp, mate_left, at(z, right), 0).start()
        hop(4, hp, mate_right, at(z, left)).wait_recv()
        hop(8, hp, mate_right, at(z, left), 1).start()

    def complete(hp):
        hop(5, hp, own_far, at(z, right), 0).wait_recv()
        hop(6, hp, own_far, at(z, left), 1).wait_recv()
        hop(7, hp, mate_far, at(z, right), 0).wait_recv()
        hop(8, hp, mate_far, at(z, left), 1).wait_recv()

    def gathered(hp, slot, which):
        blocks = []
        for k in range(CAP):
            for s in range(SRC):
                index = small[slot, k, pair * (QB * SRC) + s * QB + QB - 1]
                blocks.append(kv[hp][s, which, index])
        return blocks

    def wide_bias(bias):
        return jnp.concatenate([bias[k * QB : (k + 1) * QB] for k in range(CAP)], axis=1)

    base = 5 + 2 * pair - 3 * odd

    def partial_copies(hp, slot, k):
        row = base + slot
        return (
            remote(o_out.at[hp, slot], o_in.at[hp, k], o_send.at[slot, hp], o_recv.at[k, hp],
                   at(row, x)),
            remote(s_out.at[hp, slot], s_in.at[hp, k], s_send.at[slot, hp], s_recv.at[k, hp],
                   at(row, x)),
        )

    def visitors(hp):
        @pl.loop(0, SLOTS)
        def _(slot):
            @pl.when(base + slot < ZS)
            def _():
                if hp == 0:
                    for ref, i in ((got_bias, 0), (got_table, 1)):
                        remote(ref.at[slot], ref.at[slot], m_send.at[0, i], m_recv.at[slot, i],
                               mate).wait_recv()
                    copy = pltpu.make_async_copy(
                        got_table.at[slot], small.at[slot], small_sem.at[slot]
                    )
                    copy.start()
                    copy.wait()
                q_ref = q_buf.at[hp, slot]
                remote(q_ref, q_ref, q_send.at[0, hp], q_recv.at[slot, hp], mate).wait_recv()
                keys = jnp.concatenate(gathered(hp, slot, 0), axis=0)
                values = jnp.concatenate(gathered(hp, slot, 1), axis=0)
                bias = wide_bias(got_bias[slot])

                def masked(scores):
                    scores = scores.reshape(QB, BLOCK, LISTED) + bias[:, None, :]
                    return scores.reshape(ROWS, LISTED)

                numerator, sums, peak = attend(q_ref[...], keys, values, masked)
                o_out[hp, slot] = (numerator / sums).astype(jnp.bfloat16)
                s_out[hp, slot] = compact(peak, sums)
                for copy in partial_copies(hp, slot, pair):
                    copy.start()

    def own_queries(hp):
        if hp == 0:
            own_small.wait()
        keys = jnp.concatenate(gathered(hp, SLOTS, 0) + [kv[hp][own, 0].reshape(ROWS, PAIR)], axis=0)
        values = jnp.concatenate(gathered(hp, SLOTS, 1) + [kv[hp][own, 1].reshape(ROWS, PAIR)], axis=0)
        bias = wide_bias(pair_bias[pair])

        def masked(scores):
            others = scores[:, :LISTED].reshape(QB, BLOCK, LISTED) + bias[:, None, :]
            mine = scores[:, LISTED:] + own_bias[...]
            return jnp.concatenate([others.reshape(ROWS, LISTED), mine], axis=1)

        numerator, sums, peak = attend(q_buf[hp, SLOTS], keys, values, masked)
        own_o[hp] = numerator / sums
        own_s[hp] = compact(peak, sums)

    def att_copy(hp, side):
        part = att.at[side, hp]
        return remote(part, part, send.at[9, hp], recv.at[9, hp], mate)

    def merge(hp):
        for k in range(SLOTS):
            @pl.when(pair > k)
            def _():
                for ref, sem in ((o_in, o_recv), (s_in, s_recv)):
                    part = ref.at[hp, k]
                    remote(part, part, o_send.at[0, hp], sem.at[k, hp], mate).wait_recv()
        stats = [own_s[hp]] + [s_in[hp, k] for k in range(SLOTS)]
        shares = [[None, None] for _ in stats]
        for h in range(2):
            peaks = [s[2 * h : 2 * h + 1] for s in stats]
            top = functools.reduce(jnp.maximum, peaks)
            weights = [
                s[2 * h + 1 : 2 * h + 2] * jnp.exp(p - top) for s, p in zip(stats, peaks)
            ]
            scale = 1.0 / functools.reduce(jnp.add, weights)
            for i, w in enumerate(weights):
                shares[i][h] = w * scale
        rows = [jnp.broadcast_to(s, (16, ROWS)) for share in shares for s in share]
        turned = jnp.concatenate(rows, axis=0).T
        in_first = iota((ROWS, PAIR), 1) < HEAD_DIM
        total = jnp.zeros((ROWS, PAIR), jnp.float32)
        for i in range(1 + SLOTS):
            share = jnp.where(
                in_first, turned[:, i * 32 : i * 32 + 1], turned[:, i * 32 + 16 : i * 32 + 17]
            )
            part = own_o[hp] if i == 0 else o_in[hp, i - 1].astype(jnp.float32)
            total = total + share * part
        att[core, hp] = total.astype(jnp.bfloat16)
        att_copy(hp, core).start()

    pass_mate(0)
    relay_own(0)
    send_own(2)
    relay_mate(0)
    pass_mate(1)
    relay_own(1)
    send_own(3)
    for hp in range(HP):
        complete(hp)
        visitors(hp)
        if hp + 1 < HP:
            relay_mate(hp + 1)
        if hp + 2 < HP:
            pass_mate(hp + 2)
            relay_own(hp + 2)
        own_queries(hp)
        if hp:
            merge(hp - 1)
    merge(HP - 1)

    for hp in range(HP):
        att_copy(hp, 1 - core).wait_recv()
    loads[7].wait()
    attended = jnp.concatenate([att[s, hp] for s in range(2) for hp in range(HP)], axis=1)
    stores = []
    for c in range(ow.shape[1] // 256):
        cols = pl.ds(c * 256, 256)
        out_buf[:, cols] = jnp.dot(
            attended, ow[:, cols], preferred_element_type=jnp.float32
        ).astype(jnp.bfloat16)
        store = pltpu.make_async_copy(
            out_buf.at[:, cols], out_hbm.at[:, cols], out_sem.at[c]
        )
        store.start()
        stores.append(store)

    tokens.wait_send()
    for hp in range(HP):
        hop(0, hp, own, at(other_row, x)).wait_send()
        hop(1, hp, own, at(z, right)).wait_send()
        hop(2, hp, own, at(z, left)).wait_send()
        hop(3, hp, mated, at(z, right)).wait_send()
        hop(4, hp, mated, at(z, left)).wait_send()
        hop(5, hp, own_left, at(z, right), 0).wait_send()
        hop(6, hp, own_right, at(z, left), 1).wait_send()
        hop(7, hp, mate_left, at(z, right), 0).wait_send()
        hop(8, hp, mate_right, at(z, left), 1).wait_send()
        att_copy(hp, core).wait_send()
    for k in range(SLOTS):
        @pl.when(pair > k)
        def _():
            for copy in meta_copies(k, q_slot[k]):
                copy.wait_send()
            for hp in range(HP):
                q_copy(k, hp, q_slot[k]).wait_send()

    @pl.loop(0, SLOTS)
    def _(slot):
        @pl.when(base + slot < ZS)
        def _():
            for hp in range(HP):
                for copy in partial_copies(hp, slot, pair):
                    copy.wait_send()

    for store in stores:
        store.wait()


def on_device(tokens, query_weight, key_weight, value_weight, out_weight, chosen):
    rows, half_d = tokens.shape
    width = query_weight.shape[1]
    out_half = out_weight.shape[1]
    row_table, device_table = tables()
    bf16, f32, i32 = jnp.bfloat16, jnp.float32, jnp.int32
    vmem = pltpu.VMEM
    dma = pltpu.SemaphoreType.DMA
    scratch = [vmem((SRC, 2, QB, BLOCK, PAIR), bf16) for _ in range(HP)] + [
        vmem((2, rows, half_d), bf16),
        vmem(query_weight.shape, bf16),
        vmem(key_weight.shape, bf16),
        vmem(value_weight.shape, bf16),
        vmem(out_weight.shape, bf16),
        vmem(chosen.shape, i32),
        vmem(row_table.shape, f32),
        vmem(device_table.shape, f32),
        vmem((2, ROWS, PAIR), f32),
        vmem((3, width // 256, ROWS, 256), f32),
        vmem((QB, ROWS), f32),
        vmem((ROWS, ROWS), f32),
        vmem((4, CAP * QB, OUT_KEYS), f32),
        vmem((QB, ROWS), i32),
        vmem((SLOTS, CAP * QB, OUT_KEYS), f32),
        vmem((SLOTS, QB, ROWS), i32),
        vmem((HP, SLOTS + 1, ROWS, PAIR), bf16),
        vmem((HP, SLOTS, ROWS, PAIR), bf16),
        vmem((HP, SLOTS, 8, ROWS), f32),
        vmem((HP, SLOTS, ROWS, PAIR), bf16),
        vmem((HP, SLOTS, 8, ROWS), f32),
        vmem((HP, ROWS, PAIR), f32),
        vmem((HP, 8, ROWS), f32),
        vmem((2, HP, ROWS, PAIR), bf16),
        vmem((rows, out_half), bf16),
        pltpu.SMEM((SLOTS + 1, QB, ROWS), i32),
        dma((8,)),
        dma((10, HP)),
        dma((10, HP)),
        dma((2,)),
        dma((SLOTS, HP)),
        dma((SLOTS, HP)),
        dma((SLOTS, 2)),
        dma((SLOTS, 2)),
        dma((SLOTS, HP)),
        dma((SLOTS, HP)),
        dma((SLOTS, HP)),
        dma((SLOTS, HP)),
        dma((SLOTS + 1,)),
        dma((out_half // 256,)),
    ]
    return pl.pallas_call(
        kernel,
        out_shape=jax.ShapeDtypeStruct((rows, out_half), bf16),
        in_specs=[pl.BlockSpec(memory_space=pl.ANY)] * 8,
        out_specs=pl.BlockSpec(memory_space=pl.ANY),
        scratch_shapes=scratch,
        compiler_params=pltpu.CompilerParams(
            collective_id=0, has_side_effects=True, vmem_limit_bytes=58 * 1024 * 1024
        ),
        name="block_attention",
    )(
        tokens, query_weight, key_weight, value_weight, out_weight, chosen,
        jnp.asarray(row_table), jnp.asarray(device_table),
    )


def solution(mesh):
    placed = (
        P(DP_KV, "tp"),
        P(None, "tp"),
        P(None, "tp"),
        P(None, "tp"),
        P(None, "tp"),
        P(DP_KV, None),
    )
    return jax.shard_map(
        on_device, mesh=mesh, in_specs=placed, out_specs=P(DP_KV, "tp"), check_vma=False
    )
```

time: 278 us -> 69.2 us (0.25)
  waiting for transfers between devices: 108 us -> 0 us
  Pallas kernels: 0 us -> 67.2 us
  local copies, waits for them, and re-layouts: 52.3 us -> 1.87 us
  matrix products: 42.7 us -> 0 us
  starting transfers between devices: 33 us -> 0 us
  other arithmetic: 31.5 us -> 0 us
  blocking collectives: 7.48 us -> 0 us
    all_to_all x5 -> x0, waiting for transfers between devices: 108 us -> none  [the longest x1 66 us: on_device(): lax.all_to_all(key_store[incoming], KV, split_axis=0, concat_axis=0, tile...]
    pallas_call x0 -> x1, Pallas kernels: none -> 67.2 us  [on_device(): pl.pallas_call(kernel, out_shape=jax.ShapeDtypeStruct((rows, out_half), b...]
    dot_general x20 -> x0, matrix products: 42.7 us -> none  [the longest x8 17.1 us: one_head(): jnp.dot(weights.astype(jnp.bfloat16), value_head, preferred_element_type=...]
    all_to_all x5 -> x0, starting transfers between devices: 33 us -> none  [the longest x2 10.5 us: moved_by_axis(): whole = lax.all_to_all(whole, axes[k], k, k, tiled=True)]
    concatenate x4 -> x0, local copies, waits for them, and re-layouts: 18.2 us -> none  [the longest x2 9.22 us: on_device(): jnp.concatenate([value_proj, got_values.reshape(-1, head_width)], axis=0)]
    unnamed x30 -> x1, local copies, waits for them, and re-layouts: 16.4 us -> 1.87 us
    transpose x3 -> x0, other arithmetic: 12.9 us -> none  [the longest x1 6.42 us: attend_keys(): key_rows.reshape(key_count, head_count, HEAD_DIM).transpose(1, 0, 2)]
    reduce_sum x9 -> x0, other arithmetic: 10.1 us -> none  [the longest x8 10.1 us: one_head(): denominator = denominator * factor + jnp.sum(weights, axis=1)]
  transfers between devices with their start and end apart: 5 -> 0, of which waited for: 3 -> 0; matrix products, arithmetic and copies ran while one was open for 18% -> 0% of each run, Pallas kernels for 0% -> 0%
where the time goes in v1:
time: 69.2 us; the launch traced here: 69 us
  Pallas kernels  67.2 us (97%)
  local copies, waits for them, and re-layouts  1.87 us (3%)
    pallas_call x1, Pallas kernels, on_device(): pl.pallas_call(kernel, out_shape=jax.ShapeDtypeStruct((rows, out_half), b...  67.2 us
    unnamed x1, local copies, waits for them, and re-layouts  1.87 us

profile of v1, /device:TPU:1, one launch (start us, length us, event | category | flops | bytes accessed | tf_op | source)
XLA Modules:
  0.0 69.0 jit_solution(16787323868668141379)
XLA Ops:
  0.0 67.2 %block_attention.1 = bf16[256,1024]{1,0:T(8,128)(2,1)} custom-call(bf16[256,1024]{1,0:T(8,128)(2,1)} %tok_hbm.1, bf16[2048,512]{1,0:T(8,128)(2,1)} %wq_hbm.1, bf16[2048,512]{1,0:T(8,128)(2,1)} %wk_hbm.1, bf16[2048,512]{1,0:T(8,128)(2,1)} %wv_hbm.1, bf16[1024,1024]{1,0:T(8,128)(2,1)} %ow_hbm.1, s32[8,16]{1,0:T(8,128)} %ch_hbm.1, ...), custom_call_target="tpu_custom_call" | custom-call | tf_op jit(solution)/shard_map/block_attention/pallas_call | solution.py:534
  67.2 1.9 %copy.10 = bf16[256,1024]{1,0:T(8,128)(2,1)} copy(bf16[256,1024]{1,0:T(8,128)(2,1)} %block_attention.1) | data formatting | bytes 1048576

commit v2 on v1

--- a/solution.py
+++ b/solution.py
@@ -89,7 +89,7 @@
     kv = scratch[:HP]
     (
         tok, wq, wk, wv, ow, ch, tab, dev, angle, acc, listing, own_bias, pair_bias, table,
-        got_bias, got_table, q_buf, o_out, s_out, o_in, s_in, own_o, own_s, att, out_buf, small,
+        got_bias, got_table, q_buf, o_out, s_out, o_in, s_in, own_o, own_s, att, out_buf, out_acc, small,
         load_sem, send, recv, tok_sem, q_send, q_recv, m_send, m_recv, o_send, o_recv,
         s_send, s_recv, small_sem, out_sem,
     ) = scratch[HP:]
@@ -113,7 +113,7 @@
     loads = [
         pltpu.make_async_copy(a, b, load_sem.at[i]) for i, (a, b) in enumerate(loads)
     ]
-    for i in (4, 0, 1, 2, 3, 5, 6, 7):
+    for i in (0, 1, 2, 3, 5, 6, 4, 7):
         loads[i].start()
 
     barrier = pltpu.get_barrier_semaphore()
@@ -126,6 +126,33 @@
     greet(at(z, right))
     for k in range(1, ZS):
         greet(at((z + k) % ZS, x))
+
+    loads[5].wait()
+    loads[6].wait()
+    dev_cos, dev_sin = dev[me, 0:1, :], dev[me, 1:2, :]
+    sign = jnp.where(iota((1, PAIR), 1) % HEAD_DIM < 32, -1.0, 1.0)
+    angle[0] = tab[0] * dev_cos - tab[1] * dev_sin
+    angle[1] = (tab[1] * dev_cos + tab[0] * dev_sin) * sign
+
+    def remote(src, dst, send_sem, recv_sem, device):
+        return pltpu.make_async_remote_copy(
+            src_ref=src, dst_ref=dst, send_sem=send_sem, recv_sem=recv_sem,
+            device_id=device, device_id_type=MESH,
+        )
+
+    loads[0].wait()
+    for w, load in ((0, 1), (1, 2), (2, 3)):
+        loads[load].wait()
+        weight = (wk, wv, wq)[w]
+        for c in range(width // 256):
+            cols = pl.ds(c * 256, 256)
+            acc[w, c] = jnp.dot(
+                tok[core], weight[pl.ds(core * half_d, half_d), cols],
+                preferred_element_type=jnp.float32,
+            )
+    pl.semaphore_wait(barrier, 3 + ZS - 1)
+    tokens = remote(tok.at[core], tok.at[core], tok_sem.at[0], tok_sem.at[1], mate)
+    tokens.start()
 
     loads[4].wait()
     lane = iota((QB, ROWS), 1)
@@ -169,13 +196,6 @@
         causal = iota((BLOCK, ROWS), 1) <= iota((BLOCK, ROWS), 0) + b * BLOCK
         own_bias[rows, :] = jnp.where(causal, listing[b : b + 1, :], MASKED)
 
-    loads[5].wait()
-    loads[6].wait()
-    dev_cos, dev_sin = dev[me, 0:1, :], dev[me, 1:2, :]
-    sign = jnp.where(iota((1, PAIR), 1) % HEAD_DIM < 32, -1.0, 1.0)
-    angle[0] = tab[0] * dev_cos - tab[1] * dev_sin
-    angle[1] = (tab[1] * dev_cos + tab[0] * dev_sin) * sign
-
     for k in range(SLOTS):
         @pl.when(pair <= k)
         def _():
@@ -183,26 +203,6 @@
                 o_in[hp, k] = jnp.zeros((ROWS, PAIR), jnp.bfloat16)
                 s_in[hp, k] = jnp.full((8, ROWS), MASKED, jnp.float32)
 
-    def remote(src, dst, send_sem, recv_sem, device):
-        return pltpu.make_async_remote_copy(
-            src_ref=src, dst_ref=dst, send_sem=send_sem, recv_sem=recv_sem,
-            device_id=device, device_id_type=MESH,
-        )
-
-    pl.semaphore_wait(barrier, 3 + ZS - 1)
-    loads[0].wait()
-    tokens = remote(tok.at[core], tok.at[core], tok_sem.at[0], tok_sem.at[1], mate)
-    tokens.start()
-
-    for w, load in ((0, 1), (1, 2), (2, 3)):
-        loads[load].wait()
-        weight = (wk, wv, wq)[w]
-        for c in range(width // 256):
-            cols = pl.ds(c * 256, 256)
-            acc[w, c] = jnp.dot(
-                tok[core], weight[pl.ds(core * half_d, half_d), cols],
-                preferred_element_type=jnp.float32,
-            )
     theirs = remote(tok.at[1 - core], tok.at[1 - core], tok_sem.at[0], tok_sem.at[1], mate)
     theirs.wait_recv()
 
@@ -254,6 +254,15 @@
             remote(table, got_table.at[slot], m_send.at[k, 1], m_recv.at[slot, 1],
                    at(q_row[k], x)),
         )
+
+    def send_queries(hp):
+        for k in range(SLOTS):
+            @pl.when(pair > k)
+            def _():
+                if hp == 0:
+                    for copy in meta_copies(k, q_slot[k]):
+                        copy.start()
+                q_copy(k, hp, q_slot[k]).start()
 
     for c in range(width // 256):
         keys, values = project(0, c), project(1, c)
@@ -262,23 +271,19 @@
             part = slice(i * PAIR, (i + 1) * PAIR)
             kv[hp][own, 0] = blocked(turn(keys[:, part]))
             kv[hp][own, 1] = blocked(values[:, part])
-            send_across(hp)
-            if hp < 2:
+            if i == 0:
+                send_across(hp)
+            if c == 0:
                 send_own(hp)
-    for c in range(width // 256):
         queries = project(2, c)
         for i in range(2):
             hp = 2 * c + i
             part = slice(i * PAIR, (i + 1) * PAIR)
             turned = turn(queries[:, part]).astype(jnp.bfloat16).astype(jnp.float32)
             q_buf[hp, SLOTS] = (turned * HEAD_DIM**-0.5).astype(jnp.bfloat16)
-            for k in range(SLOTS):
-                @pl.when(pair > k)
-                def _():
-                    if hp == 0:
-                        for copy in meta_copies(k, q_slot[k]):
-                            copy.start()
-                    q_copy(k, hp, q_slot[k]).start()
+            send_queries(hp)
+            if i == 0:
+                send_across(hp + 1)
 
     own_small = pltpu.make_async_copy(table, small.at[SLOTS], small_sem.at[SLOTS])
     own_small.start()
@@ -413,6 +418,25 @@
         att[core, hp] = total.astype(jnp.bfloat16)
         att_copy(hp, core).start()
 
+    def project_out(hp):
+        att_copy(hp, 1 - core).wait_recv()
+        if hp == 0:
+            loads[7].wait()
+        heads = jnp.concatenate([att[s, hp] for s in range(2)], axis=1)
+        outs = []
+        for c in range(ow.shape[1] // 256):
+            cols = pl.ds(c * 256, 256)
+            weight = jnp.concatenate(
+                [ow[pl.ds(s * width + hp * PAIR, PAIR), cols] for s in range(2)], axis=0
+            )
+            out = jnp.dot(heads, weight, preferred_element_type=jnp.float32)
+            if hp:
+                out = out + out_acc[c]
+            if hp < HP - 1:
+                out_acc[c] = out
+            outs.append(out)
+        return outs
+
     pass_mate(0)
     relay_own(0)
     send_own(2)
@@ -431,18 +455,15 @@
         own_queries(hp)
         if hp:
             merge(hp - 1)
+        if hp > 1:
+            project_out(hp - 2)
     merge(HP - 1)
-
-    for hp in range(HP):
-        att_copy(hp, 1 - core).wait_recv()
-    loads[7].wait()
-    attended = jnp.concatenate([att[s, hp] for s in range(2) for hp in range(HP)], axis=1)
+    project_out(HP - 2)
+
     stores = []
-    for c in range(ow.shape[1] // 256):
+    for c, out in enumerate(project_out(HP - 1)):
         cols = pl.ds(c * 256, 256)
-        out_buf[:, cols] = jnp.dot(
-            attended, ow[:, cols], preferred_element_type=jnp.float32
-        ).astype(jnp.bfloat16)
+        out_buf[:, cols] = out.astype(jnp.bfloat16)
         store = pltpu.make_async_copy(
             out_buf.at[:, cols], out_hbm.at[:, cols], out_sem.at[c]
         )
@@ -515,6 +536,7 @@
         vmem((HP, 8, ROWS), f32),
         vmem((2, HP, ROWS, PAIR), bf16),
         vmem((rows, out_half), bf16),
+        vmem((out_half // 256, rows, 256), f32),
         pltpu.SMEM((SLOTS + 1, QB, ROWS), i32),
         dma((8,)),
         dma((10, HP)),

time: 69.2 us -> 63.7 us (0.921)
  Pallas kernels: 67.2 us -> 61.7 us
    pallas_call x1, Pallas kernels: 67.2 us -> 61.7 us  [on_device(): pl.pallas_call(kernel, out_shape=jax.ShapeDtypeStruct((rows, out_half), b...]
where the time goes in v2:
time: 63.7 us; the launch traced here: 63.6 us
  Pallas kernels  61.7 us (97%)
  local copies, waits for them, and re-layouts  1.87 us (3%)
    pallas_call x1, Pallas kernels, on_device(): pl.pallas_call(kernel, out_shape=jax.ShapeDtypeStruct((rows, out_half), b...  61.7 us
    unnamed x1, local copies, waits for them, and re-layouts  1.87 us

profile of v2, /device:TPU:1, one launch (start us, length us, event | category | flops | bytes accessed | tf_op | source)
XLA Modules:
  0.0 63.6 jit_solution(9546350642712674511)
XLA Ops:
  0.0 61.7 %block_attention.1 = bf16[256,1024]{1,0:T(8,128)(2,1)} custom-call(bf16[256,1024]{1,0:T(8,128)(2,1)} %tok_hbm.1, bf16[2048,512]{1,0:T(8,128)(2,1)} %wq_hbm.1, bf16[2048,512]{1,0:T(8,128)(2,1)} %wk_hbm.1, bf16[2048,512]{1,0:T(8,128)(2,1)} %wv_hbm.1, bf16[1024,1024]{1,0:T(8,128)(2,1)} %ow_hbm.1, s32[8,16]{1,0:T(8,128)} %ch_hbm.1, ...), custom_call_target="tpu_custom_call" | custom-call | tf_op jit(solution)/shard_map/block_attention/pallas_call | solution.py:556
  61.7 1.9 %copy.10 = bf16[256,1024]{1,0:T(8,128)(2,1)} copy(bf16[256,1024]{1,0:T(8,128)(2,1)} %block_attention.1) | data formatting | bytes 1048576

commit v3 on v2

--- a/solution.py
+++ b/solution.py
@@ -75,12 +75,17 @@
 def compact(peak, sums):
     lane = iota((ROWS, PAIR), 1)
     turned = jnp.where(lane % HEAD_DIM < 32, peak, sums).T
-    row = iota((8, ROWS), 0) % 4
-    return jnp.where(
-        row == 0,
-        turned[0:8],
-        jnp.where(row == 1, turned[32:40], jnp.where(row == 2, turned[64:72], turned[96:104])),
-    )
+    row = iota((8, PAIR), 0)
+    packed = jnp.zeros((8, PAIR), jnp.float32)
+    for k in range(4):
+        part = turned[k * 32 : k * 32 + 8]
+        packed = jnp.where(row == 2 * k, part[:, :PAIR], packed)
+        packed = jnp.where(row == 2 * k + 1, part[:, PAIR:], packed)
+    return packed
+
+
+def row_of(stats, k):
+    return jnp.concatenate([stats[2 * k : 2 * k + 1], stats[2 * k + 1 : 2 * k + 2]], axis=1)
 
 
 def kernel(
@@ -184,7 +189,7 @@
         spread = (iota((ROWS, OUT_KEYS), 0) // QB) == (iota((ROWS, OUT_KEYS), 1) // BLOCK + k * SRC)
         spread = spread.astype(jnp.float32).astype(jnp.bfloat16)
         found = jnp.dot(placed, spread, preferred_element_type=jnp.float32)
-        pair_bias[k] = (found - 1.0) * -MASKED
+        pair_bias[k] = ((found - 1.0) * -MASKED).astype(jnp.bfloat16)
     spread = iota((ROWS, ROWS), 0) == (iota((ROWS, ROWS), 1) // BLOCK + me * QB)
     spread = spread.astype(jnp.float32).astype(jnp.bfloat16)
     found = jnp.dot(
@@ -201,7 +206,7 @@
         def _():
             for hp in range(HP):
                 o_in[hp, k] = jnp.zeros((ROWS, PAIR), jnp.bfloat16)
-                s_in[hp, k] = jnp.full((8, ROWS), MASKED, jnp.float32)
+                s_in[hp, k] = jnp.full((8, PAIR), MASKED, jnp.float32)
 
     theirs = remote(tok.at[1 - core], tok.at[1 - core], tok_sem.at[0], tok_sem.at[1], mate)
     theirs.wait_recv()
@@ -238,8 +243,9 @@
     def send_across(hp):
         hop(0, hp, own, at(other_row, x)).start()
 
-    q_row = [1 - z // 5, 3 - z // 7, z * 0 + 5]
-    q_slot = [(z + 1) % 3, (z + 2) % 3, z % 2]
+    turn_back = (z - 3) // 2 - 1
+    q_row = [1 - z // 5, 3 - turn_back * turn_back, z * 0 + 5]
+    q_slot = [(z + 1) % 3, (z // 2) % 2, z % 2]
 
     def q_copy(k, hp, slot):
         return remote(
@@ -271,7 +277,7 @@
             part = slice(i * PAIR, (i + 1) * PAIR)
             kv[hp][own, 0] = blocked(turn(keys[:, part]))
             kv[hp][own, 1] = blocked(values[:, part])
-            if i == 0:
+            if hp == 0:
                 send_across(hp)
             if c == 0:
                 send_own(hp)
@@ -281,9 +287,9 @@
             part = slice(i * PAIR, (i + 1) * PAIR)
             turned = turn(queries[:, part]).astype(jnp.bfloat16).astype(jnp.float32)
             q_buf[hp, SLOTS] = (turned * HEAD_DIM**-0.5).astype(jnp.bfloat16)
-            send_queries(hp)
-            if i == 0:
-                send_across(hp + 1)
+            if hp == 0:
+                send_queries(0)
+                send_across(1)
 
     own_small = pltpu.make_async_copy(table, small.at[SLOTS], small_sem.at[SLOTS])
     own_small.start()
@@ -326,10 +332,16 @@
     def wide_bias(bias):
         return jnp.concatenate([bias[k * QB : (k + 1) * QB] for k in range(CAP)], axis=1)
 
-    base = 5 + 2 * pair - 3 * odd
+    pair3 = pair // 3
+    pair2, pair1, pair0 = (pair // 2) * (1 - pair3), (pair % 2) * (1 - pair3), (3 - pair) // 3
+    base = pair0 * (5 - 3 * odd) + pair1 * (4 + odd) + pair2 * (8 - 2 * odd) + pair3 * 8
+
+    def sender(slot):
+        return base + slot * (1 + 2 * pair1 * (1 - odd)) + (slot // 2) * 5 * pair1 * odd
+
 
     def partial_copies(hp, slot, k):
-        row = base + slot
+        row = sender(slot)
         return (
             remote(o_out.at[hp, slot], o_in.at[hp, k], o_send.at[slot, hp], o_recv.at[k, hp],
                    at(row, x)),
@@ -340,7 +352,11 @@
     def visitors(hp):
         @pl.loop(0, SLOTS)
         def _(slot):
-            @pl.when(base + slot < ZS)
+            @pl.when(slot == SLOTS - 1)
+            def _():
+                keep_ring_going(hp)
+
+            @pl.when(sender(slot) < ZS)
             def _():
                 if hp == 0:
                     for ref, i in ((got_bias, 0), (got_table, 1)):
@@ -355,7 +371,7 @@
                 remote(q_ref, q_ref, q_send.at[0, hp], q_recv.at[slot, hp], mate).wait_recv()
                 keys = jnp.concatenate(gathered(hp, slot, 0), axis=0)
                 values = jnp.concatenate(gathered(hp, slot, 1), axis=0)
-                bias = wide_bias(got_bias[slot])
+                bias = wide_bias(got_bias[slot].astype(jnp.float32))
 
                 def masked(scores):
                     scores = scores.reshape(QB, BLOCK, LISTED) + bias[:, None, :]
@@ -372,7 +388,7 @@
             own_small.wait()
         keys = jnp.concatenate(gathered(hp, SLOTS, 0) + [kv[hp][own, 0].reshape(ROWS, PAIR)], axis=0)
         values = jnp.concatenate(gathered(hp, SLOTS, 1) + [kv[hp][own, 1].reshape(ROWS, PAIR)], axis=0)
-        bias = wide_bias(pair_bias[pair])
+        bias = wide_bias(pair_bias[pair].astype(jnp.float32))
 
         def masked(scores):
             others = scores[:, :LISTED].reshape(QB, BLOCK, LISTED) + bias[:, None, :]
@@ -397,10 +413,10 @@
         stats = [own_s[hp]] + [s_in[hp, k] for k in range(SLOTS)]
         shares = [[None, None] for _ in stats]
         for h in range(2):
-            peaks = [s[2 * h : 2 * h + 1] for s in stats]
+            peaks = [row_of(s, 2 * h) for s in stats]
             top = functools.reduce(jnp.maximum, peaks)
             weights = [
-                s[2 * h + 1 : 2 * h + 2] * jnp.exp(p - top) for s, p in zip(stats, peaks)
+                row_of(s, 2 * h + 1) * jnp.exp(p - top) for s, p in zip(stats, peaks)
             ]
             scale = 1.0 / functools.reduce(jnp.add, weights)
             for i, w in enumerate(weights):
@@ -438,22 +454,31 @@
         return outs
 
     pass_mate(0)
+    send_queries(1)
     relay_own(0)
     send_own(2)
     relay_mate(0)
     pass_mate(1)
     relay_own(1)
     send_own(3)
-    for hp in range(HP):
-        complete(hp)
-        visitors(hp)
+    send_across(2)
+    send_queries(2)
+
+    def keep_ring_going(hp):
         if hp + 1 < HP:
             relay_mate(hp + 1)
         if hp + 2 < HP:
             pass_mate(hp + 2)
             relay_own(hp + 2)
+        if hp == 0:
+            send_across(3)
+            send_queries(3)
+
+    for hp in range(HP):
+        complete(hp)
+        visitors(hp)
         own_queries(hp)
-        if hp:
+        if hp :
             merge(hp - 1)
         if hp > 1:
             project_out(hp - 2)
@@ -492,7 +517,7 @@
 
     @pl.loop(0, SLOTS)
     def _(slot):
-        @pl.when(base + slot < ZS)
+        @pl.when(sender(slot) < ZS)
         def _():
             for hp in range(HP):
                 for copy in partial_copies(hp, slot, pair):
@@ -523,17 +548,17 @@
         vmem((3, width // 256, ROWS, 256), f32),
         vmem((QB, ROWS), f32),
         vmem((ROWS, ROWS), f32),
-        vmem((4, CAP * QB, OUT_KEYS), f32),
+        vmem((4, CAP * QB, OUT_KEYS), bf16),
         vmem((QB, ROWS), i32),
-        vmem((SLOTS, CAP * QB, OUT_KEYS), f32),
+        vmem((SLOTS, CAP * QB, OUT_KEYS), bf16),
         vmem((SLOTS, QB, ROWS), i32),
         vmem((HP, SLOTS + 1, ROWS, PAIR), bf16),
         vmem((HP, SLOTS, ROWS, PAIR), bf16),
-        vmem((HP, SLOTS, 8, ROWS), f32),
+        vmem((HP, SLOTS, 8, PAIR), f32),
         vmem((HP, SLOTS, ROWS, PAIR), bf16),
-        vmem((HP, SLOTS, 8, ROWS), f32),
+        vmem((HP, SLOTS, 8, PAIR), f32),
         vmem((HP, ROWS, PAIR), f32),
-        vmem((HP, 8, ROWS), f32),
+        vmem((HP, 8, PAIR), f32),
         vmem((2, HP, ROWS, PAIR), bf16),
         vmem((rows, out_half), bf16),
         vmem((out_half // 256, rows, 256), f32),

time: 63.7 us -> 61.4 us (0.964)
  Pallas kernels: 61.7 us -> 59.4 us
    pallas_call x1, Pallas kernels: 61.7 us -> 59.4 us  [on_device(): pl.pallas_call(kernel, out_shape=jax.ShapeDtypeStruct((rows, out_half), b...]
where the time goes in v3:
time: 61.4 us; the launch traced here: 61.3 us
  Pallas kernels  59.4 us (97%)
  local copies, waits for them, and re-layouts  1.87 us (3%)
    pallas_call x1, Pallas kernels, on_device(): pl.pallas_call(kernel, out_shape=jax.ShapeDtypeStruct((rows, out_half), b...  59.4 us
    unnamed x1, local copies, waits for them, and re-layouts  1.87 us

profile of v3, /device:TPU:1, one launch (start us, length us, event | category | flops | bytes accessed | tf_op | source)
XLA Modules:
  0.0 61.3 jit_solution(4243001622342058488)
XLA Ops:
  0.0 59.4 %block_attention.1 = bf16[256,1024]{1,0:T(8,128)(2,1)} custom-call(bf16[256,1024]{1,0:T(8,128)(2,1)} %tok_hbm.1, bf16[2048,512]{1,0:T(8,128)(2,1)} %wq_hbm.1, bf16[2048,512]{1,0:T(8,128)(2,1)} %wk_hbm.1, bf16[2048,512]{1,0:T(8,128)(2,1)} %wv_hbm.1, bf16[1024,1024]{1,0:T(8,128)(2,1)} %ow_hbm.1, s32[8,16]{1,0:T(8,128)} %ch_hbm.1, ...), custom_call_target="tpu_custom_call" | custom-call | tf_op jit(solution)/shard_map/block_attention/pallas_call | solution.py:581
  59.4 1.9 %copy.10 = bf16[256,1024]{1,0:T(8,128)(2,1)} copy(bf16[256,1024]{1,0:T(8,128)(2,1)} %block_attention.1) | data formatting | bytes 1048576

commit v4 on v3

--- a/solution.py
+++ b/solution.py
@@ -130,7 +130,8 @@
     greet(at(z, left))
     greet(at(z, right))
     for k in range(1, ZS):
-        greet(at((z + k) % ZS, x))
+        if k != ZS // 2:
+            greet(at((z + k) % ZS, x))
 
     loads[5].wait()
     loads[6].wait()
@@ -155,7 +156,7 @@
                 tok[core], weight[pl.ds(core * half_d, half_d), cols],
                 preferred_element_type=jnp.float32,
             )
-    pl.semaphore_wait(barrier, 3 + ZS - 1)
+    pl.semaphore_wait(barrier, 3 + ZS - 2)
     tokens = remote(tok.at[core], tok.at[core], tok_sem.at[0], tok_sem.at[1], mate)
     tokens.start()
 
@@ -434,12 +435,15 @@
         att[core, hp] = total.astype(jnp.bfloat16)
         att_copy(hp, core).start()
 
+    def out_copy(c):
+        cols = pl.ds(c * 256, 256)
+        return pltpu.make_async_copy(out_buf.at[:, cols], out_hbm.at[:, cols], out_sem.at[c])
+
     def project_out(hp):
         att_copy(hp, 1 - core).wait_recv()
         if hp == 0:
             loads[7].wait()
         heads = jnp.concatenate([att[s, hp] for s in range(2)], axis=1)
-        outs = []
         for c in range(ow.shape[1] // 256):
             cols = pl.ds(c * 256, 256)
             weight = jnp.concatenate(
@@ -450,8 +454,9 @@
                 out = out + out_acc[c]
             if hp < HP - 1:
                 out_acc[c] = out
-            outs.append(out)
-        return outs
+            else:
+                out_buf[:, cols] = out.astype(jnp.bfloat16)
+                out_copy(c).start()
 
     pass_mate(0)
     send_queries(1)
@@ -485,15 +490,7 @@
     merge(HP - 1)
     project_out(HP - 2)
 
-    stores = []
-    for c, out in enumerate(project_out(HP - 1)):
-        cols = pl.ds(c * 256, 256)
-        out_buf[:, cols] = out.astype(jnp.bfloat16)
-        store = pltpu.make_async_copy(
-            out_buf.at[:, cols], out_hbm.at[:, cols], out_sem.at[c]
-        )
-        store.start()
-        stores.append(store)
+    project_out(HP - 1)
 
     tokens.wait_send()
     for hp in range(HP):
@@ -523,8 +520,8 @@
                 for copy in partial_copies(hp, slot, pair):
                     copy.wait_send()
 
-    for store in stores:
-        store.wait()
+    for c in range(ow.shape[1] // 256):
+        out_copy(c).wait()
 
 
 def on_device(tokens, query_weight, key_weight, value_weight, out_weight, chosen):

time: 61.4 us -> 60.9 us (level)
  no operation moved by 1% of the time
where the time goes in v4:
time: 60.9 us; the launch traced here: 60.8 us
  Pallas kernels  59 us (97%)
  local copies, waits for them, and re-layouts  1.87 us (3%)
    pallas_call x1, Pallas kernels, on_device(): pl.pallas_call(kernel, out_shape=jax.ShapeDtypeStruct((rows, out_half), b...  59 us
    unnamed x1, local copies, waits for them, and re-layouts  1.87 us

profile of v4, /device:TPU:1, one launch (start us, length us, event | category | flops | bytes accessed | tf_op | source)
XLA Modules:
  0.0 60.8 jit_solution(17081133317702684026)
XLA Ops:
  0.0 59.0 %block_attention.1 = bf16[256,1024]{1,0:T(8,128)(2,1)} custom-call(bf16[256,1024]{1,0:T(8,128)(2,1)} %tok_hbm.1, bf16[2048,512]{1,0:T(8,128)(2,1)} %wq_hbm.1, bf16[2048,512]{1,0:T(8,128)(2,1)} %wk_hbm.1, bf16[2048,512]{1,0:T(8,128)(2,1)} %wv_hbm.1, bf16[1024,1024]{1,0:T(8,128)(2,1)} %ow_hbm.1, s32[8,16]{1,0:T(8,128)} %ch_hbm.1, ...), custom_call_target="tpu_custom_call" | custom-call | tf_op jit(solution)/shard_map/block_attention/pallas_call | solution.py:578
  59.0 1.9 %copy.10 = bf16[256,1024]{1,0:T(8,128)(2,1)} copy(bf16[256,1024]{1,0:T(8,128)(2,1)} %block_attention.1) | data formatting | bytes 1048576
